TPU v7x, 256 devices: a 8x8x2 block of a 8x8x16 slice. The times are simulated.
256 devices in a mesh: grp: 2 (over z), ep: 64 (over y, x), tp: 2 (over core).
Axes of the slice: x: 8, y: 8, z: 2, core: 2. Of those that a mesh axis runs over, the one named last changes fastest.
The devices are a block of a 8x8x16 slice.
Arguments:
- tokens_in: bfloat16 [8192, 2048], P(('grp', 'ep')), parts along dimension 0, may hold values from -6 to 6
- norm_gain: float32 [2048], replicated, may hold values from 0.1 to 1.9
- gate_proj: bfloat16 [64, 2048, 1024], P('ep', None, 'tp'), may hold values from -0.125 to 0.125
- up_proj: bfloat16 [64, 2048, 1024], P('ep', None, 'tp'), may hold values from -0.125 to 0.125
- down_proj: bfloat16 [64, 1024, 2048], P('ep', 'tp'), may hold values from -0.1875 to 0.1875
- route_ids: int32 [8192, 8], P(('grp', 'ep')), parts along dimension 0, may hold values from 0 to 63, all different within a row; in each aligned block of 64 rows (0 to 63, 64 to 127, ...) at most 16 rows name the same one
- group_weight: float32 [8192, 8], P(('grp', 'ep')), parts along dimension 0, may hold values from 0.05 to 1
- expert_weight: float32 [8192, 8], P(('grp', 'ep')), parts along dimension 0, may hold values from 0.05 to 1
Outputs:
- expert_mix: bfloat16 [8192, 2048], P(('grp', 'ep'), 'tp'), parts along dimension 0
There are 2 independent parts, one for each index of `grp`. A program takes and returns all parts, laid end to end along the dimension named above; an argument that names none is the same for every part. Nothing has to cross between parts.
Inputs may be any that keep to these rules, and one draw needn't show every extreme that they name: `route_ids`: each row names 8 different experts; within the rows of one index of ep no expert is named by more than 16 rows, a bound that some of them reach.
All inputs are finite; a program needn't handle non-finite values.
Results may differ from a plain program's by a relative error of at most 0.0077.
Values may be sent and summed in bfloat16 or wider, within the bound.
A program may use at most 64 MiB of HBM per device.

v0:
```python
import jax
import jax.numpy as jnp
from jax import lax
from jax.sharding import PartitionSpec as P

TOP = 8
EXP_GRP = 8


EPSILON = 1e-06


def cut_along(array, dim, size):
    lengths = array.shape
    blocks = array.reshape(*lengths[:dim], size, lengths[dim] // size, *lengths[dim + 1 :])
    return jnp.moveaxis(blocks, dim, 0)


def sum_at_owner(array, axis, dim):
    size = lax.axis_size(axis)
    blocks = lax.all_to_all(cut_along(array, dim, size), axis, 0, 0, tiled=True)
    return jnp.sum(blocks.astype(jnp.float32), axis=0)


def on_device(
    tokens_in, norm_gain, gate_proj, up_proj, down_proj, route_ids, group_weight, expert_weight
):
    token_count, model_width = tokens_in.shape
    expert_count = gate_proj.shape[0] * lax.axis_size("ep")
    lane_count = lax.axis_size("tp")
    part_width = model_width // lane_count
    capacity = min(token_count, max(2, 2 * token_count * TOP // expert_count))
    slot_total = expert_count * capacity
    row_values = tokens_in.astype(jnp.float32)
    inv_scale = lax.rsqrt(jnp.mean(row_values * row_values, axis=-1, keepdims=True) + EPSILON)
    normed = (row_values * inv_scale * norm_gain).astype(jnp.bfloat16)
    route_count = token_count * TOP
    flat_ids = route_ids.reshape(route_count)
    positions = jnp.arange(route_count, dtype=jnp.int32)
    same_expert = (flat_ids[:, None] == flat_ids[None, :]) & (
        positions[None, :] < positions[:, None]
    )
    slot_rank = jnp.sum(same_expert.astype(jnp.int32), axis=1)
    slot_index = flat_ids * capacity + slot_rank
    slot_match = jnp.arange(slot_total, dtype=jnp.int32)[:, None] == slot_index[None, :]
    selector = jnp.sum(
        slot_match.reshape(slot_total, token_count, TOP).astype(jnp.int32), axis=2
    ).astype(jnp.bfloat16)
    gate_local = gate_proj[0]
    up_local = up_proj[0]
    lane_index = lax.axis_index("tp")
    own_half = lax.dynamic_slice_in_dim(normed, lane_index * part_width, part_width, 1)
    outgoing = jnp.dot(selector, own_half, preferred_element_type=jnp.float32).astype(jnp.bfloat16)
    arrived = lax.all_to_all(
        outgoing.reshape(expert_count, capacity, part_width),
        "ep",
        split_axis=0,
        concat_axis=0,
        tiled=True,
    )
    arrived = arrived.reshape(slot_total, part_width)
    column_piece = lax.all_gather(arrived, "tp", axis=1, tiled=True)
    gate_acts = jnp.dot(column_piece, gate_local, preferred_element_type=jnp.float32)
    up_acts = jnp.dot(column_piece, up_local, preferred_element_type=jnp.float32)
    hidden = (jax.nn.silu(gate_acts) * up_acts).astype(jnp.bfloat16)
    partial_rows = jnp.dot(hidden, down_proj[0], preferred_element_type=jnp.float32)
    summed = sum_at_owner(
        partial_rows.reshape(expert_count, capacity, model_width).astype(jnp.bfloat16), "tp", 2
    )
    results = summed.astype(jnp.bfloat16)
    returned = lax.all_to_all(results, "ep", split_axis=0, concat_axis=0, tiled=True).reshape(
        slot_total, part_width
    )
    picked = returned[slot_index].astype(jnp.float32).reshape(token_count, TOP, part_width)
    group_ids = route_ids // EXP_GRP
    group_count = group_weight.shape[1]
    group_match = (
        group_ids[:, :, None] == jnp.arange(group_count, dtype=jnp.int32)[None, None, :]
    ).astype(jnp.float32)
    group_part = jnp.sum(group_weight[:, None, :] * group_match, axis=2)
    gate_values = group_part * expert_weight / jnp.sum(expert_weight, axis=1, keepdims=True)
    return jnp.sum(picked * gate_values[:, :, None], axis=1).astype(jnp.bfloat16)


def solution(mesh):
    in_specs = (
        P(("grp", "ep"), None),
        P(),
        P("ep", None, "tp"),
        P("ep", None, "tp"),
        P("ep", "tp", None),
        P(("grp", "ep"), None),
        P(("grp", "ep"), None),
        P(("grp", "ep"), None),
    )
    out_specs = P(("grp", "ep"), "tp")
    return jax.shard_map(
        on_device, mesh=mesh, in_specs=in_specs, out_specs=out_specs, check_vma=False
    )
```

profile of v0, /device:TPU:513, one launch (start us, length us, event | category | flops | bytes accessed | tf_op | source)
XLA Modules:
  0.0 214.2 jit_solution(7506265072580166607)
XLA Ops:
  6.5 0.0 copy-start
  6.6 0.0 all-gather.2.cloned.1.call-start
  6.6 1.1 convert_element_type.40
  7.7 1.1 multiply_reduce_fusion
  8.8 0.8 copy.24
  9.6 0.1 eq.43
  9.7 0.3 convert_reduce_fusion.1
  9.9 0.1 reduce_sum.71
  10.0 0.7 convert_reduce_fusion
  10.7 0.7 dynamic-slice
  11.4 0.8 convolution_convert_fusion.1
  12.2 65.2 %all_to_all.15 = bf16[64,16,1024]{2,1,0:T(8,128)(2,1)} all-to-all(bf16[64,16,1024]{2,1,0:T(8,128)(2,1)S(1)} %bitcast.33), channel_id=1, replica_groups=mesh['grp'=2,'ep'=64,'tp'=2] {'ep'}, dimensions={0} | all-to-all | bytes 4194304 | tf_op jit(solution)/shard_map/all_to_all | solution.py:54
  77.4 0.1 all-gather.2.cloned.1.call-update
  77.4 37.4 %all-gather.2.cloned.1.call-done = bf16[1024,2048]{1,0:T(8,128)(2,1)} async-done(((bf16[1024,1024]{1,0:T(8,128)(2,1)}), bf16[1024,2048]{1,0:T(8,128)(2,1)}) %all-gather.2.cloned.1.call-update) | async-done | bytes 4194320 | tf_op jit(solution)/shard_map/all_gather | solution.py:62
  114.9 5.3 %fusion.2 = f32[1024,512]{1,0:T(8,128)S(1)} fusion(bf16[1024,2048]{1,0:T(8,128)(2,1)} %all-gather.2.cloned.1.call-done, bf16[1,2048,512]{2,1,0:T(8,128)(2,1)} %param.11), kind=kOutput, calls=%fused_computation.6 | convolution fusion | flops 2147483648 | bytes 8388608 | tf_op jit(solution)/shard_map/dot_general | solution.py:64
  120.2 0.0 copy-done.4
  120.2 0.0 copy-done.5
  120.2 2.7 %multiply_convert_fusion = bf16[1024,512]{1,0:T(8,128)(2,1)S(1)} fusion(f32[1024,512]{1,0:T(8,128)S(1)} %fusion.2, bf16[1024,2048]{1,0:T(8,128)(2,1)S(1)} %copy-done.4, bf16[1,2048,512]{2,1,0:T(8,128)(2,1)S(1)} %copy-done.5), kind=kOutput, calls=%fused_computation.10 | convolution fusion | flops 2150629376 | bytes 9437184 | tf_op jit(solution)/shard_map/dot_general | solution.py:63
  122.9 0.0 copy-done
  122.9 2.3 %convolution_convert_fusion = bf16[64,16,2048]{2,1,0:T(8,128)(2,1)S(1)} fusion(bf16[64,16,512]{2,1,0:T(8,128)(2,1)S(1)} %bitcast.37, bf16[1,512,2048]{2,1,0:T(8,128)(2,1)S(1)} %copy-done), kind=kOutput, calls=%fused_computation.2 | convolution fusion | flops 2149580800 | bytes 7340032 | tf_op jit(solution)/shard_map/dot_general | solution.py:66
  125.2 0.6 copy.30
  125.9 8.0 %all_to_all.16 = bf16[2,64,16,1024]{3,2,1,0:T(8,128)(2,1)} all-to-all(bf16[2,64,16,1024]{3,2,1,0:T(8,128)(2,1)S(1)} %bitcast.31), channel_id=1, replica_groups=mesh['grp'=2,'ep'=64,'tp'=2] {'tp'}, dimensions={0} | all-to-all | bytes 8388608 | tf_op jit(solution)/shard_map/all_to_all | solution.py:21
  133.9 5.2 %reduce_sum.74 = bf16[64,16,1024]{2,1,0:T(8,128)(2,1)} reduce(bf16[2,64,16,1024]{3,2,1,0:T(8,128)(2,1)} %all_to_all.16, bf16[]{:T(256)} %constant.37.clone.1), dimensions={0}, to_apply=%region_3.4 | reduce | flops 1048576 | bytes 6291458 | tf_op jit(solution)/shard_map/reduce_sum | solution.py:22
  139.1 13.5 %all-to-all-start.2 = ((bf16[64,16,1024]{2,1,0:T(8,128)(2,1)}), bf16[64,16,1024]{2,1,0:T(8,128)(2,1)}, u32[]{:S(2)}, u32[]{:S(2)}) async-start(bf16[64,16,1024]{2,1,0:T(8,128)(2,1)} %reduce_sum.74), calls=%async_computation.2 | async-start | bytes 4194304 | tf_op jit(solution)/shard_map/all_to_all | solution.py:71
  152.6 0.1 mul.78
  152.7 0.0 copy-done.1
  152.8 0.0 copy-done.2
  152.8 0.0 copy-done.3
  152.8 0.1 copy.27
  152.9 48.4 %all-to-all-done.2 = bf16[64,16,1024]{2,1,0:T(8,128)(2,1)} async-done(((bf16[64,16,1024]{2,1,0:T(8,128)(2,1)}), bf16[64,16,1024]{2,1,0:T(8,128)(2,1)}, u32[]{:S(2)}, u32[]{:S(2)}) %all-to-all-start.2) | async-done | bytes 2097184 | tf_op jit(solution)/shard_map/all_to_all | solution.py:71
  201.4 4.6 %gather_fusion = bf16[512,1024]{1,0:T(8,128)(2,1)S(1)} fusion(bf16[1024,1024]{1,0:T(8,128)(2,1)} %bitcast.8, s32[1024]{0:T(1024)S(1)} %pad_clamp_fusion), kind=kCustom, calls=%fused_computation | custom fusion | bytes 2099200 | tf_op jit(solution)/shard_map/gather | solution.py:74
  206.0 1.4 fusion
  (13 shorter events, 0.1 us)
Async XLA Ops:
  6.5 116.3 %copy-start = (bf16[1,512,2048]{2,1,0:T(8,128)(2,1)S(1)}, bf16[1,512,2048]{2,1,0:T(8,128)(2,1)}, u32[]{:S(2)}) copy-start(bf16[1,512,2048]{2,1,0:T(8,128)(2,1)} %param.12) | copy-start | bytes 6291460
  6.6 108.3 %all-gather.2.cloned.1.call-start = ((), (), s32[]{:S(2)}) async-start(), calls=%async_computation.3 | async-start | bytes 6291456 | tf_op jit(solution)/shard_map/all_gather | solution.py:62
  114.9 5.3 %copy-start.4 = (bf16[1024,2048]{1,0:T(8,128)(2,1)S(1)}, bf16[1024,2048]{1,0:T(8,128)(2,1)}, u32[]{:S(2)}) copy-start(bf16[1024,2048]{1,0:T(8,128)(2,1)} %all-gather.2.cloned.1.call-done) | copy-start | bytes 12582916
  114.9 5.3 %copy-start.5 = (bf16[1,2048,512]{2,1,0:T(8,128)(2,1)S(1)}, bf16[1,2048,512]{2,1,0:T(8,128)(2,1)}, u32[]{:S(2)}) copy-start(bf16[1,2048,512]{2,1,0:T(8,128)(2,1)} %param.10) | copy-start | bytes 6291460
  139.1 13.6 %copy-start.1 = (f32[64,8]{0,1:T(8,128)S(1)}, f32[64,8]{0,1:T(8,128)}, u32[]{:S(2)}) copy-start(f32[64,8]{0,1:T(8,128)} %param.15) | copy-start | bytes 6148
  139.1 13.6 %copy-start.2 = (s32[64,8]{0,1:T(8,128)S(1)}, s32[64,8]{0,1:T(8,128)}, u32[]{:S(2)}) copy-start(s32[64,8]{0,1:T(8,128)} %param.13) | copy-start | bytes 6148
  139.1 13.7 %copy-start.3 = (f32[64,8]{0,1:T(8,128)S(1)}, f32[64,8]{0,1:T(8,128)}, u32[]{:S(2)}) copy-start(f32[64,8]{0,1:T(8,128)} %param.14) | copy-start | bytes 6148
  139.1 62.2 %all-to-all-start.2 = ((bf16[64,16,1024]{2,1,0:T(8,128)(2,1)}), bf16[64,16,1024]{2,1,0:T(8,128)(2,1)}, u32[]{:S(2)}, u32[]{:S(2)}) async-start(bf16[64,16,1024]{2,1,0:T(8,128)(2,1)} %reduce_sum.74), calls=%async_computation.2 | async-start | bytes 4194304 | tf_op jit(solution)/shard_map/all_to_all | solution.py:71
Sparse Core Ops, SparseCore 0:
  77.6 37.2 all-gather.1
where the time goes:
time: 216 us; the launch traced here: 214 us
  waiting for transfers between devices  85.9 us (40%)
  blocking collectives  73.2 us (34%)
  between operations  13.6 us (6%)
  starting transfers between devices  13.5 us (6%)
  matrix products  11.1 us (5%)
  other arithmetic  9.82 us (5%)
  local copies, waits for them, and re-layouts  7.08 us (3%)
    all_to_all x1, blocking collectives, on_device(): lax.all_to_all(outgoing.reshape(expert_count, capacity, part_width), 'ep'...  65.2 us
    all_to_all x1, waiting for transfers between devices, on_device(): lax.all_to_all(results, 'ep', split_axis=0, concat_axis=0, tiled=True)  48.4 us
    all_gather x1, waiting for transfers between devices, on_device(): column_piece = lax.all_gather(arrived, 'tp', axis=1, tiled=True)  37.4 us
    all_to_all x1, starting transfers between devices, on_device(): lax.all_to_all(results, 'ep', split_axis=0, concat_axis=0, tiled=True)  13.5 us
    all_to_all x1, blocking collectives, sum_at_owner(): blocks = lax.all_to_all(cut_along(array, dim, size), axis, 0, 0, tiled=True)  8.03 us
    dot_general x1, matrix products, on_device(): jnp.dot(column_piece, up_local, preferred_element_type=jnp.float32)  5.32 us
    reduce_sum x1, other arithmetic, sum_at_owner(): return jnp.sum(blocks.astype(jnp.float32), axis=0)  5.22 us
    gather x1, local copies, waits for them, and re-layouts, on_device(): returned[slot_index].astype(jnp.float32)  4.59 us
  transfers between devices with their start and end apart: 2, of which 2 were waited for; matrix products, arithmetic and copies ran while one was open for 0% of the time, Pallas kernels for 0%

commit v1 on v0

v1 whole, which is shorter than its diff:
```python
import functools
import math

import jax
import jax.numpy as jnp
from jax import lax
from jax.experimental import pallas as pl
from jax.experimental.pallas import tpu as pltpu
from jax.sharding import PartitionSpec as P

TOP = 8
EXP_GRP = 8
EPSILON = 1e-06
MESH = pl.DeviceIdType.MESH
SIDE = 8
BF = jnp.bfloat16
F32 = jnp.float32

OFF = [0, 1, 7, 2, 6, 3, 5, 4]
BACK = [OFF.index((-o) % SIDE) for o in OFF]
INWARD = [7, 5, 6, 3, 4, 1, 2, 0]


def ring_offset(place):
    half = (place + 1) // 2
    odd = place % 2
    return (odd * half + (1 - odd) * (SIDE - half)) % SIDE


def moe_kernel(
    routes_ref, tokens_hbm, gain_ref, gate_hbm, up_hbm, down_hbm, out_ref,
    tok_in, toks, meta_out, meta, sel, xin, xoth, wg, wu, wd, accg, accu, hid,
    part_out, part_own, part_in, res, ret, sums_out, sums_in,
    load_sem, ag_send, ag_recv, meta_send, meta_recv, sel_send, xin_recv, xo_send, xo_recv,
    part_send, part_recv, res_send, ret_recv, sum_send, sum_recv,
):
    rows, width = tok_in.shape
    part = width // 2
    cap = sel.shape[2]
    hidden = wg.shape[2]
    grp = lax.axis_index("grp")
    ep = lax.axis_index("ep")
    core = lax.axis_index("tp")
    up_y = ep // SIDE
    up_x = ep % SIDE
    first = up_x * (1 - core) + up_y * core
    second = up_y * (1 - core) + up_x * core
    step_first = (1 - core) + SIDE * core
    step_second = SIDE * (1 - core) + core

    def along_first(place):
        at = (first + OFF[place]) % SIDE
        return (grp, at * step_first + second * step_second, core)

    def along_second(place):
        at = (second + OFF[place]) % SIDE
        return (grp, first * step_first + at * step_second, core)

    partner = (grp, ep, 1 - core)

    barrier = pltpu.get_barrier_semaphore()
    for place in range(1, SIDE):
        pl.semaphore_signal(barrier, inc=1, device_id=along_first(place), device_id_type=MESH)
        pl.semaphore_signal(barrier, inc=1, device_id=along_second(place), device_id_type=MESH)
    pl.semaphore_signal(barrier, inc=1, device_id=partner, device_id_type=MESH)

    def send(src, dst, send_sem, recv_sem, to):
        copy = pltpu.make_async_remote_copy(
            src_ref=src, dst_ref=dst, send_sem=send_sem, recv_sem=recv_sem,
            device_id=to, device_id_type=MESH,
        )
        copy.start()

    def wait_bytes(ref, sem):
        pltpu.make_async_copy(ref, ref, sem).wait()

    own = pl.ds(pl.multiple_of(core * part, part), part)
    other = pl.ds(pl.multiple_of((1 - core) * part, part), part)
    tok_load = pltpu.make_async_copy(tokens_hbm, tok_in, load_sem.at[0])
    tok_load.start()
    loads = [
        pltpu.make_async_copy(gate_hbm.at[0, own], wg.at[0], load_sem.at[1]),
        pltpu.make_async_copy(up_hbm.at[0, own], wu.at[0], load_sem.at[2]),
        pltpu.make_async_copy(gate_hbm.at[0, other], wg.at[1], load_sem.at[3]),
        pltpu.make_async_copy(up_hbm.at[0, other], wu.at[1], load_sem.at[4]),
        pltpu.make_async_copy(down_hbm.at[0, :, own], wd.at[0], load_sem.at[5]),
        pltpu.make_async_copy(down_hbm.at[0, :, other], wd.at[1], load_sem.at[6]),
    ]
    for load in loads:
        load.start()

    lanes = 2 * rows
    experts = SIDE * SIDE
    row = lax.broadcasted_iota(jnp.int32, (experts, lanes), 0)
    lane = lax.broadcasted_iota(jnp.int32, (experts, lanes), 1)
    at_first = (first + ring_offset(row // SIDE)) % SIDE
    at_second = (second + ring_offset(row % SIDE)) % SIDE
    expert = at_first * step_first + at_second * step_second
    weight_sum = jnp.sum(routes_ref[2 * TOP : 3 * TOP, :], axis=0, keepdims=True)
    named = jnp.zeros((experts, lanes), F32)
    weight = jnp.zeros((experts, lanes), F32)
    expert_f = expert.astype(F32)
    for k in range(TOP):
        match = expert_f == routes_ref[k : k + 1, :]
        named = jnp.where(match, 1.0, named)
        weight = jnp.where(match, routes_ref[2 * TOP + k : 2 * TOP + k + 1, :], weight)
    group = expert // EXP_GRP
    group_part = jnp.zeros((experts, lanes), F32)
    for g in range(experts // EXP_GRP):
        group_part = jnp.where(group == g, routes_ref[TOP + g : TOP + g + 1, :], group_part)
    gates = group_part * weight / weight_sum
    high = gates.astype(BF).astype(F32)
    gates = jnp.where(lane < rows, high, gates - high)
    before = lax.broadcasted_iota(jnp.int32, (lanes, lanes), 0)
    after = lax.broadcasted_iota(jnp.int32, (lanes, lanes), 1)
    earlier = jnp.where((before < after) & (before // rows == after // rows), 1.0, 0.0).astype(BF)
    rank = jnp.dot(named.astype(BF), earlier, preferred_element_type=F32)
    slots = jnp.where(named > 0.0, rank, -1.0)
    meta_out[:, 0] = slots.reshape(SIDE, SIDE, lanes)
    meta_out[:, 1] = gates.reshape(SIDE, SIDE, lanes)
    meta[0] = meta_out[0]

    tok_load.wait()
    values = tok_in[...].astype(F32)
    scale = lax.rsqrt(jnp.mean(values * values, axis=-1, keepdims=True) + EPSILON)
    toks[0] = (tok_in[:, own].astype(F32) * scale * gain_ref[:, own]).astype(BF)

    accg[...] = jnp.zeros_like(accg)
    accu[...] = jnp.zeros_like(accu)

    pl.semaphore_wait(barrier, 2 * (SIDE - 1) + 1)

    def pass_on(place, to_place):
        toward = BACK[1] if OFF[to_place] < SIDE // 2 else BACK[2]
        send(toks.at[place], toks.at[to_place], ag_send.at[to_place], ag_recv.at[to_place], along_first(toward))

    pass_on(0, 1)
    pass_on(0, 2)
    for place in range(1, SIDE):
        send(meta_out.at[place], meta.at[BACK[place]], meta_send.at[place], meta_recv.at[BACK[place]], along_first(place))

    slot_iota = (lax.broadcasted_iota(jnp.int32, (SIDE * cap, lanes), 0) % cap).astype(F32)

    def spread(table):
        return jnp.concatenate(
            [jnp.broadcast_to(table[j : j + 1, :], (cap, lanes)) for j in range(SIDE)], axis=0
        )

    def pick_and_send(s):
        if s > 0:
            wait_bytes(toks.at[s], ag_recv.at[s])
            if s % 2 == 1 and s < 5:
                pass_on(s, s + 2)
            elif s in (2, 4):
                pass_on(s, s + 2)
            elif s == 6:
                pass_on(s, 7)
            wait_bytes(meta.at[s], meta_recv.at[s])
        chosen = jnp.where(spread(meta[s, 0]) == slot_iota, 1.0, 0.0).astype(BF)[:, :rows]
        picked = jnp.dot(chosen, toks[s], preferred_element_type=F32).astype(BF)
        picked = picked.reshape(SIDE, cap, part)
        sel[s] = picked
        xin[s, 0] = picked[0]
        for place in range(SIDE - 1, 0, -1):
            send(sel.at[s, place], xin.at[s, BACK[place]], sel_send.at[s], xin_recv.at[s], along_second(place))

    def take_own(s):
        wait_bytes(xin.at[s, pl.ds(1, SIDE - 1)], xin_recv.at[s])
        send(xin.at[s], xoth.at[:, s], xo_send.at[s], xo_recv.at[s], partner)
        block = xin[s].reshape(SIDE * cap, part)
        accg[s] += jnp.dot(block, wg[0], preferred_element_type=F32).reshape(SIDE, cap, hidden)
        accu[s] += jnp.dot(block, wu[0], preferred_element_type=F32).reshape(SIDE, cap, hidden)

    def take_other(s):
        wait_bytes(xoth.at[:, s], xo_recv.at[s])
        block = xoth[:, s].reshape(SIDE * cap, part)
        accg[:, s] += jnp.dot(block, wg[1], preferred_element_type=F32).reshape(SIDE, cap, hidden)
        accu[:, s] += jnp.dot(block, wu[1], preferred_element_type=F32).reshape(SIDE, cap, hidden)

    for step in range(SIDE + 3):
        if step == 2:
            for load in loads:
                load.wait()
        if step < SIDE:
            pick_and_send(step)
        if 2 <= step < SIDE + 2:
            take_own(step - 2)
        if 3 <= step:
            take_other(step - 3)

    for s in range(SIDE):
        gate_acts = accg[s]
        hid[s] = (gate_acts / (1.0 + jnp.exp(-gate_acts)) * accu[s]).astype(BF)

    def multiply_down(s):
        theirs = hid[:, s].reshape(SIDE * cap, hidden)
        part_out[s] = jnp.dot(theirs, wd[1], preferred_element_type=F32).astype(BF).reshape(SIDE, cap, part)
        send(part_out.at[s], part_in.at[s], part_send.at[s], part_recv.at[s], partner)
        mine = hid[s].reshape(SIDE * cap, hidden)
        part_own[s] = jnp.dot(mine, wd[0], preferred_element_type=F32).astype(BF).reshape(SIDE, cap, part)

    def return_rows(s):
        wait_bytes(part_in.at[s], part_recv.at[s])
        res[s] = (part_own[s].astype(F32) + part_in[s].astype(F32)).astype(BF)
        ret[s, 0] = res[s, 0]
        for place in range(SIDE - 1, 0, -1):
            send(res.at[s, place], ret.at[s, BACK[place]], res_send.at[s], ret_recv.at[s], along_second(place))

    def mix(s):
        wait_bytes(ret.at[s, pl.ds(1, SIDE - 1)], ret_recv.at[s])
        mixer = jnp.where(spread(meta[s, 0]) == slot_iota, spread(meta[s, 1]), 0.0).astype(BF)
        both = lax.dot_general(
            mixer, ret[s].reshape(SIDE * cap, part), (((0,), (0,)), ((), ())), preferred_element_type=F32
        )
        total = both[:rows] + both[rows:]
        arriving = [s] if s in (1, 2, 3, 4, 5) else ([0, 6] if s == 0 else [])
        for slot in arriving:
            wait_bytes(sums_in.at[slot], sum_recv.at[slot])
            total = total + sums_in[slot].astype(F32)
        if s == 0:
            out_ref[...] = total.astype(BF)
            return
        sums_out[s] = total.astype(BF)
        to_slot = {7: 5, 5: 3, 3: 1, 1: 0, 6: 4, 4: 2, 2: 6}[s]
        toward = 1 if s % 2 == 1 else 2
        send(sums_out.at[s], sums_in.at[to_slot], sum_send.at[s], sum_recv.at[to_slot], along_first(toward))

    for step in range(SIDE + 3):
        if step < SIDE:
            multiply_down(INWARD[step])
        if 1 <= step < SIDE + 1:
            return_rows(INWARD[step - 1])
        if 3 <= step:
            mix(INWARD[step - 3])

    for place in range(1, SIDE):
        wait_bytes(toks.at[place], ag_send.at[place])
        wait_bytes(meta_out.at[place], meta_send.at[place])
        wait_bytes(sums_out.at[place], sum_send.at[place])
    for s in range(SIDE):
        wait_bytes(sel.at[s, pl.ds(1, SIDE - 1)], sel_send.at[s])
        wait_bytes(xin.at[s], xo_send.at[s])
        wait_bytes(part_out.at[s], part_send.at[s])
        wait_bytes(res.at[s, pl.ds(1, SIDE - 1)], res_send.at[s])


def on_device(
    tokens_in, norm_gain, gate_proj, up_proj, down_proj, route_ids, group_weight, expert_weight
):
    rows, width = tokens_in.shape
    experts = gate_proj.shape[0] * lax.axis_size("ep")
    hidden = gate_proj.shape[2]
    cap = min(rows, max(2, 2 * rows * TOP // experts))
    part = width // 2
    routes = jnp.concatenate(
        [route_ids.astype(F32), group_weight, expert_weight], axis=1
    ).T
    routes = jnp.concatenate([routes, routes], axis=1)
    vmem = lambda *shape: pltpu.VMEM(shape, BF)
    dma = pltpu.SemaphoreType.DMA
    blocks = (SIDE, SIDE, cap, part)
    return pl.pallas_call(
        moe_kernel,
        out_shape=jax.ShapeDtypeStruct((rows, part), BF),
        in_specs=[
            pl.BlockSpec(memory_space=pltpu.VMEM),
            pl.BlockSpec(memory_space=pl.ANY),
            pl.BlockSpec(memory_space=pltpu.VMEM),
            pl.BlockSpec(memory_space=pl.ANY),
            pl.BlockSpec(memory_space=pl.ANY),
            pl.BlockSpec(memory_space=pl.ANY),
        ],
        out_specs=pl.BlockSpec(memory_space=pltpu.VMEM),
        scratch_shapes=[
            vmem(rows, width),
            vmem(SIDE, rows, part),
            pltpu.VMEM((SIDE, 2, SIDE, 2 * rows), F32),
            pltpu.VMEM((SIDE, 2, SIDE, 2 * rows), F32),
            vmem(*blocks),
            vmem(*blocks),
            vmem(*blocks),
            vmem(2, part, hidden),
            vmem(2, part, hidden),
            vmem(2, hidden, part),
            pltpu.VMEM((SIDE, SIDE, cap, hidden), F32),
            pltpu.VMEM((SIDE, SIDE, cap, hidden), F32),
            vmem(SIDE, SIDE, cap, hidden),
            vmem(*blocks),
            vmem(*blocks),
            vmem(*blocks),
            vmem(*blocks),
            vmem(*blocks),
            vmem(SIDE, rows, part),
            vmem(SIDE, rows, part),
            dma((7,)),
        ]
        + [dma((SIDE,)) for _ in range(14)],
        compiler_params=pltpu.CompilerParams(
            collective_id=0, has_side_effects=True, vmem_limit_bytes=60 * 1024 * 1024
        ),
        name="moe",
    )(routes, tokens_in, norm_gain.reshape(1, width), gate_proj, up_proj, down_proj)


def solution(mesh):
    in_specs = (
        P(("grp", "ep"), None),
        P(),
        P("ep", None, "tp"),
        P("ep", None, "tp"),
        P("ep", "tp", None),
        P(("grp", "ep"), None),
        P(("grp", "ep"), None),
        P(("grp", "ep"), None),
    )
    out_specs = P(("grp", "ep"), "tp")
    return jax.shard_map(
        on_device, mesh=mesh, in_specs=in_specs, out_specs=out_specs, check_vma=False
    )
```

time: 216 us -> 99.4 us (0.46)
  Pallas kernels: 0 us -> 94.6 us
  waiting for transfers between devices: 85.9 us -> 0 us
  blocking collectives: 73.2 us -> 0 us
  between operations: 13.6 us -> 0.01 us
  starting transfers between devices: 13.5 us -> 0 us
  matrix products: 11.1 us -> 0 us
  other arithmetic: 9.82 us -> 2.07 us
  local copies, waits for them, and re-layouts: 7.08 us -> 1.57 us
    pallas_call x0 -> x1, Pallas kernels: none -> 94.6 us  [on_device(): pl.pallas_call(moe_kernel, out_shape=jax.ShapeDtypeStruct((rows, part), B...]
    all_to_all x2 -> x0, blocking collectives: 73.2 us -> none  [the longest x1 65.2 us: on_device(): lax.all_to_all(outgoing.reshape(expert_count, capacity, part_width), 'ep'...]
    all_to_all x1 -> x0, waiting for transfers between devices: 48.4 us -> none  [on_device(): lax.all_to_all(results, 'ep', split_axis=0, concat_axis=0, tiled=True)]
    all_gather x1 -> x0, waiting for transfers between devices: 37.4 us -> none  [on_device(): column_piece = lax.all_gather(arrived, 'tp', axis=1, tiled=True)]
    all_to_all x1 -> x0, starting transfers between devices: 13.5 us -> none  [on_device(): lax.all_to_all(results, 'ep', split_axis=0, concat_axis=0, tiled=True)]
    dot_general x4 -> x0, matrix products: 11.1 us -> none  [the longest x1 5.32 us: on_device(): jnp.dot(column_piece, up_local, preferred_element_type=jnp.float32)]
    reduce_sum x7 -> x0, other arithmetic: 8.65 us -> none  [the longest x1 5.22 us: sum_at_owner(): return jnp.sum(blocks.astype(jnp.float32), axis=0)]
    gather x1 -> x0, local copies, waits for them, and re-layouts: 4.59 us -> none  [on_device(): returned[slot_index].astype(jnp.float32)]
  transfers between devices with their start and end apart: 2 -> 0, of which waited for: 2 -> 0; matrix products, arithmetic and copies ran while one was open for 0% -> 0% of each run, Pallas kernels for 0% -> 0%
where the time goes in v1:
time: 99.4 us; the launch traced here: 98.2 us
  Pallas kernels  94.6 us (95%)
  other arithmetic  2.07 us (2%)
  local copies, waits for them, and re-layouts  1.57 us (2%)
    pallas_call x1, Pallas kernels, on_device(): pl.pallas_call(moe_kernel, out_shape=jax.ShapeDtypeStruct((rows, part), B...  94.6 us

profile of v1, /device:TPU:513, one launch (start us, length us, event | category | flops | bytes accessed | tf_op | source)
XLA Modules:
  0.0 98.2 jit_solution(700929875652019060)
XLA Ops:
  0.0 0.7 convert_element_type.3
  0.7 0.7 maximum_bitcast_fusion
  1.4 0.7 pad_maximum_fusion.routes_ref
  2.1 94.6 %moe.1 = bf16[64,1024]{1,0:T(8,128)(2,1)} custom-call(f32[24,128]{1,0:T(8,128)} %pad_maximum_fusion.routes_ref, bf16[64,2048]{1,0:T(8,128)(2,1)} %tokens_hbm.1, f32[1,2048]{1,0:T(1,128)} %bitcast.3, bf16[1,2048,512]{2,1,0:T(8,128)(2,1)} %gate_hbm.1, bf16[1,2048,512]{2,1,0:T(8,128)(2,1)} %up_hbm.1, bf16[1,512,2048]{2,1,0:T(8,128)(2,1)} %down_hbm.1), custom_call_target="tpu_custom_call" | custom-call | tf_op jit(solution)/shard_map/moe/pallas_call | solution.py:262
  96.7 1.6 %copy.10 = bf16[64,1024]{1,0:T(8,128)(2,1)} copy(bf16[64,1024]{1,0:T(8,128)(2,1)} %moe.1) | data formatting | bytes 262144

commit v2 on v1

--- a/solution.py
+++ b/solution.py
@@ -18,7 +18,36 @@
 
 OFF = [0, 1, 7, 2, 6, 3, 5, 4]
 BACK = [OFF.index((-o) % SIDE) for o in OFF]
-INWARD = [7, 5, 6, 3, 4, 1, 2, 0]
+FAR = SIDE - 1
+OUTWARD = [
+    ((0,), (), ()),
+    ((1, 2), (), ()),
+    ((3, 4), (0, 1), ()),
+    ((5, 6), (2, 3), (0, 1)),
+    ((FAR,), (4, 5, 6, FAR), (2, 3, 4, 5, 6, FAR)),
+]
+INWARD_GROUPS = [(FAR,), (5, 6), (3, 4), (1, 2), (0,)]
+INWARD = [s for places in INWARD_GROUPS for s in places]
+RING_CUT = 4
+SUM_CUT = 2
+
+
+def next_outward(place, p):
+    if place + 2 < FAR:
+        return place + 2
+    return FAR if place == (6, 5)[p % 2] else None
+
+
+def next_inward(place, p):
+    if place == FAR:
+        return ((5, 1), (6, 2))[p % 2]
+    return {1: 0, 2: 6 + 1}.get(place, place - 2), 2 - place % 2
+
+
+def sums_from(place, p):
+    if place in (5, 6):
+        return (place,) if place == (5, 6)[p % 2] else ()
+    return {0: (0, 7), FAR: ()}.get(place, (place,))
 
 
 def ring_offset(place):
@@ -28,11 +57,11 @@
 
 
 def moe_kernel(
-    routes_ref, tokens_hbm, gain_ref, gate_hbm, up_hbm, down_hbm, out_ref,
+    ids_ref, group_ref, weight_ref, tokens_hbm, gain_ref, gate_hbm, up_hbm, down_hbm, out_ref,
     tok_in, toks, meta_out, meta, sel, xin, xoth, wg, wu, wd, accg, accu, hid,
-    part_out, part_own, part_in, res, ret, sums_out, sums_in,
-    load_sem, ag_send, ag_recv, meta_send, meta_recv, sel_send, xin_recv, xo_send, xo_recv,
-    part_send, part_recv, res_send, ret_recv, sum_send, sum_recv,
+    part_out, part_own, part_in, res, ret, sums_out, sums_in, mixed,
+    load_sem, ag_send, ag_recv, sum_send, sum_recv, meta_send, meta_recv, sel_send, xin_recv, xo_send, xo_recv,
+    part_send, part_recv, res_send, ret_recv,
 ):
     rows, width = tok_in.shape
     part = width // 2
@@ -96,18 +125,24 @@
     at_first = (first + ring_offset(row // SIDE)) % SIDE
     at_second = (second + ring_offset(row % SIDE)) % SIDE
     expert = at_first * step_first + at_second * step_second
-    weight_sum = jnp.sum(routes_ref[2 * TOP : 3 * TOP, :], axis=0, keepdims=True)
+
+    def across(ref):
+        turned = ref[...].astype(F32)
+        return jnp.concatenate([turned, turned], axis=1)
+
+    ids, group_weights, weights = across(ids_ref), across(group_ref), across(weight_ref)
+    weight_sum = jnp.sum(weights, axis=0, keepdims=True)
     named = jnp.zeros((experts, lanes), F32)
     weight = jnp.zeros((experts, lanes), F32)
     expert_f = expert.astype(F32)
     for k in range(TOP):
-        match = expert_f == routes_ref[k : k + 1, :]
+        match = expert_f == ids[k : k + 1, :]
         named = jnp.where(match, 1.0, named)
-        weight = jnp.where(match, routes_ref[2 * TOP + k : 2 * TOP + k + 1, :], weight)
+        weight = jnp.where(match, weights[k : k + 1, :], weight)
     group = expert // EXP_GRP
     group_part = jnp.zeros((experts, lanes), F32)
     for g in range(experts // EXP_GRP):
-        group_part = jnp.where(group == g, routes_ref[TOP + g : TOP + g + 1, :], group_part)
+        group_part = jnp.where(group == g, group_weights[g : g + 1, :], group_part)
     gates = group_part * weight / weight_sum
     high = gates.astype(BF).astype(F32)
     gates = jnp.where(lane < rows, high, gates - high)
@@ -130,14 +165,21 @@
 
     pl.semaphore_wait(barrier, 2 * (SIDE - 1) + 1)
 
-    def pass_on(place, to_place):
-        toward = BACK[1] if OFF[to_place] < SIDE // 2 else BACK[2]
-        send(toks.at[place], toks.at[to_place], ag_send.at[to_place], ag_recv.at[to_place], along_first(toward))
-
-    pass_on(0, 1)
-    pass_on(0, 2)
+    def piece(p):
+        return pl.ds(p * (rows // RING_CUT), rows // RING_CUT)
+
+    def pass_on(place, to_place, p):
+        backward = place % 2 == 1 if place else to_place % 2 == 1
+        send(
+            toks.at[place, piece(p)], toks.at[to_place, piece(p)],
+            ag_send.at[to_place, p], ag_recv.at[to_place, p], along_first(2 if backward else 1),
+        )
+
     for place in range(1, SIDE):
         send(meta_out.at[place], meta.at[BACK[place]], meta_send.at[place], meta_recv.at[BACK[place]], along_first(place))
+    for p in range(RING_CUT):
+        pass_on(0, 1, p)
+        pass_on(0, 2, p)
 
     slot_iota = (lax.broadcasted_iota(jnp.int32, (SIDE * cap, lanes), 0) % cap).astype(F32)
 
@@ -146,15 +188,17 @@
             [jnp.broadcast_to(table[j : j + 1, :], (cap, lanes)) for j in range(SIDE)], axis=0
         )
 
+    def receive(places):
+        for p in range(RING_CUT):
+            for s in places:
+                if s > 0:
+                    wait_bytes(toks.at[s, piece(p)], ag_recv.at[s, p])
+                    onward = next_outward(s, p)
+                    if onward:
+                        pass_on(s, onward, p)
+
     def pick_and_send(s):
         if s > 0:
-            wait_bytes(toks.at[s], ag_recv.at[s])
-            if s % 2 == 1 and s < 5:
-                pass_on(s, s + 2)
-            elif s in (2, 4):
-                pass_on(s, s + 2)
-            elif s == 6:
-                pass_on(s, 7)
             wait_bytes(meta.at[s], meta_recv.at[s])
         chosen = jnp.where(spread(meta[s, 0]) == slot_iota, 1.0, 0.0).astype(BF)[:, :rows]
         picked = jnp.dot(chosen, toks[s], preferred_element_type=F32).astype(BF)
@@ -177,16 +221,17 @@
         accg[:, s] += jnp.dot(block, wg[1], preferred_element_type=F32).reshape(SIDE, cap, hidden)
         accu[:, s] += jnp.dot(block, wu[1], preferred_element_type=F32).reshape(SIDE, cap, hidden)
 
-    for step in range(SIDE + 3):
-        if step == 2:
+    for places, owns, others in OUTWARD:
+        receive(places)
+        for s in places:
+            pick_and_send(s)
+        if places == (3, 4):
             for load in loads:
                 load.wait()
-        if step < SIDE:
-            pick_and_send(step)
-        if 2 <= step < SIDE + 2:
-            take_own(step - 2)
-        if 3 <= step:
-            take_other(step - 3)
+        for s in owns:
+            take_own(s)
+        for s in others:
+            take_other(s)
 
     for s in range(SIDE):
         gate_acts = accg[s]
@@ -206,37 +251,48 @@
         for place in range(SIDE - 1, 0, -1):
             send(res.at[s, place], ret.at[s, BACK[place]], res_send.at[s], ret_recv.at[s], along_second(place))
 
-    def mix(s):
+    columns = part // SUM_CUT
+
+    def mix(s, at):
         wait_bytes(ret.at[s, pl.ds(1, SIDE - 1)], ret_recv.at[s])
         mixer = jnp.where(spread(meta[s, 0]) == slot_iota, spread(meta[s, 1]), 0.0).astype(BF)
         both = lax.dot_general(
             mixer, ret[s].reshape(SIDE * cap, part), (((0,), (0,)), ((), ())), preferred_element_type=F32
         )
-        total = both[:rows] + both[rows:]
-        arriving = [s] if s in (1, 2, 3, 4, 5) else ([0, 6] if s == 0 else [])
-        for slot in arriving:
-            wait_bytes(sums_in.at[slot], sum_recv.at[slot])
-            total = total + sums_in[slot].astype(F32)
+        mixed[at] = both[:rows] + both[rows:]
+
+    def pass_sum(s, at, p):
+        total = mixed[at, :, p * columns : (p + 1) * columns]
+        for slot in sums_from(s, p):
+            wait_bytes(sums_in.at[slot, p], sum_recv.at[slot, p])
+            total = total + sums_in[slot, p].astype(F32)
         if s == 0:
-            out_ref[...] = total.astype(BF)
+            out_ref[:, p * columns : (p + 1) * columns] = total
             return
-        sums_out[s] = total.astype(BF)
-        to_slot = {7: 5, 5: 3, 3: 1, 1: 0, 6: 4, 4: 2, 2: 6}[s]
-        toward = 1 if s % 2 == 1 else 2
-        send(sums_out.at[s], sums_in.at[to_slot], sum_send.at[s], sum_recv.at[to_slot], along_first(toward))
-
-    for step in range(SIDE + 3):
+        sums_out[s, p] = total.astype(BF)
+        to_slot, toward = next_inward(s, p)
+        send(
+            sums_out.at[s, p], sums_in.at[to_slot, p], sum_send.at[s, p], sum_recv.at[to_slot, p], along_first(toward)
+        )
+
+    for step in range(SIDE + 1):
         if step < SIDE:
             multiply_down(INWARD[step])
-        if 1 <= step < SIDE + 1:
+        if 1 <= step:
             return_rows(INWARD[step - 1])
-        if 3 <= step:
-            mix(INWARD[step - 3])
+    for places in INWARD_GROUPS:
+        for at, s in enumerate(places):
+            mix(s, at)
+        for p in range(SUM_CUT):
+            for at, s in enumerate(places):
+                pass_sum(s, at, p)
 
     for place in range(1, SIDE):
-        wait_bytes(toks.at[place], ag_send.at[place])
         wait_bytes(meta_out.at[place], meta_send.at[place])
-        wait_bytes(sums_out.at[place], sum_send.at[place])
+        for p in range(RING_CUT):
+            wait_bytes(toks.at[place, piece(p)], ag_send.at[place, p])
+        for p in range(SUM_CUT):
+            wait_bytes(sums_out.at[place, p], sum_send.at[place, p])
     for s in range(SIDE):
         wait_bytes(sel.at[s, pl.ds(1, SIDE - 1)], sel_send.at[s])
         wait_bytes(xin.at[s], xo_send.at[s])
@@ -252,17 +308,15 @@
     hidden = gate_proj.shape[2]
     cap = min(rows, max(2, 2 * rows * TOP // experts))
     part = width // 2
-    routes = jnp.concatenate(
-        [route_ids.astype(F32), group_weight, expert_weight], axis=1
-    ).T
-    routes = jnp.concatenate([routes, routes], axis=1)
     vmem = lambda *shape: pltpu.VMEM(shape, BF)
     dma = pltpu.SemaphoreType.DMA
     blocks = (SIDE, SIDE, cap, part)
-    return pl.pallas_call(
+    result = pl.pallas_call(
         moe_kernel,
-        out_shape=jax.ShapeDtypeStruct((rows, part), BF),
+        out_shape=jax.ShapeDtypeStruct((rows, part), F32),
         in_specs=[
+            pl.BlockSpec(memory_space=pltpu.VMEM),
+            pl.BlockSpec(memory_space=pltpu.VMEM),
             pl.BlockSpec(memory_space=pltpu.VMEM),
             pl.BlockSpec(memory_space=pl.ANY),
             pl.BlockSpec(memory_space=pltpu.VMEM),
@@ -290,16 +344,25 @@
             vmem(*blocks),
             vmem(*blocks),
             vmem(*blocks),
-            vmem(SIDE, rows, part),
-            vmem(SIDE, rows, part),
+            vmem(SIDE, SUM_CUT, rows, part // SUM_CUT),
+            vmem(SIDE, SUM_CUT, rows, part // SUM_CUT),
+            pltpu.VMEM((2, rows, part), F32),
             dma((7,)),
+            dma((SIDE, RING_CUT)),
+            dma((SIDE, RING_CUT)),
+            dma((SIDE, SUM_CUT)),
+            dma((SIDE, SUM_CUT)),
         ]
-        + [dma((SIDE,)) for _ in range(14)],
+        + [dma((SIDE,)) for _ in range(10)],
         compiler_params=pltpu.CompilerParams(
             collective_id=0, has_side_effects=True, vmem_limit_bytes=60 * 1024 * 1024
         ),
         name="moe",
-    )(routes, tokens_in, norm_gain.reshape(1, width), gate_proj, up_proj, down_proj)
+    )(
+        route_ids.T, group_weight.T, expert_weight.T,
+        tokens_in, norm_gain.reshape(1, width), gate_proj, up_proj, down_proj,
+    )
+    return result.astype(BF)
 
 
 def solution(mesh):

time: 99.4 us -> 96.2 us (0.968); the launches traced: 98.2 us -> 96.1 us
  local copies, waits for them, and re-layouts: 1.57 us -> 0 us
    unnamed x1 -> x0, local copies, waits for them, and re-layouts: 1.57 us -> none
where the time goes in v2:
time: 96.2 us; the launch traced here: 96.1 us
  Pallas kernels  94.4 us (98%)
  other arithmetic  1.62 us (2%)
    pallas_call x1, Pallas kernels, on_device(): pl.pallas_call(moe_kernel, out_shape=jax.ShapeDtypeStruct((rows, part), F...  94.4 us

profile of v2, /device:TPU:513, one launch (start us, length us, event | category | flops | bytes accessed | tf_op | source)
XLA Modules:
  0.0 96.1 jit_solution(15777351599758061767)
XLA Ops:
  0.0 94.4 %moe.1 = f32[64,1024]{1,0:T(8,128)} custom-call(s32[8,64]{1,0:T(8,128)} %bitcast.5, f32[8,64]{1,0:T(8,128)} %bitcast.6, f32[8,64]{1,0:T(8,128)} %bitcast.7, bf16[64,2048]{1,0:T(8,128)(2,1)} %tokens_hbm.1, f32[1,2048]{1,0:T(1,128)} %bitcast.4, bf16[1,2048,512]{2,1,0:T(8,128)(2,1)} %gate_hbm.1, bf16[1,2048,512]{2,1,0:T(8,128)(2,1)} %up_hbm.1, ...), custom_call_target="tpu_custom_call" | custom-call | tf_op jit(solution)/shard_map/moe/pallas_call | solution.py:314
  94.5 1.6 %convert_element_type.3 = bf16[64,1024]{1,0:T(8,128)(2,1)} convert(f32[64,1024]{1,0:T(8,128)} %moe.1) | non-fusion elementwise | flops 65536 | bytes 393216 | tf_op jit(solution)/shard_map/convert_element_type | solution.py:365

commit v3 on v2

--- a/solution.py
+++ b/solution.py
@@ -19,13 +19,6 @@
 OFF = [0, 1, 7, 2, 6, 3, 5, 4]
 BACK = [OFF.index((-o) % SIDE) for o in OFF]
 FAR = SIDE - 1
-OUTWARD = [
-    ((0,), (), ()),
-    ((1, 2), (), ()),
-    ((3, 4), (0, 1), ()),
-    ((5, 6), (2, 3), (0, 1)),
-    ((FAR,), (4, 5, 6, FAR), (2, 3, 4, 5, 6, FAR)),
-]
 INWARD_GROUPS = [(FAR,), (5, 6), (3, 4), (1, 2), (0,)]
 INWARD = [s for places in INWARD_GROUPS for s in places]
 RING_CUT = 4
@@ -61,7 +54,7 @@
     tok_in, toks, meta_out, meta, sel, xin, xoth, wg, wu, wd, accg, accu, hid,
     part_out, part_own, part_in, res, ret, sums_out, sums_in, mixed,
     load_sem, ag_send, ag_recv, sum_send, sum_recv, meta_send, meta_recv, sel_send, xin_recv, xo_send, xo_recv,
-    part_send, part_recv, res_send, ret_recv,
+    part_send, part_recv, res_send, ret_recv, lead_sem,
 ):
     rows, width = tok_in.shape
     part = width // 2
@@ -87,11 +80,29 @@
 
     partner = (grp, ep, 1 - core)
 
+    peer_count = 2 * (SIDE - 1) + 1
+    in_lead_row = (second == 0) & (core == 0)
+    in_lead_column = (first == 0) & (core == 0)
+    is_lead = in_lead_row & in_lead_column
+    beside_lead = (ep == 0) & (core == 1)
+    knows_lead = (in_lead_row | in_lead_column | beside_lead) & jnp.logical_not(is_lead)
+
+    def signal_peers(semaphore):
+        for place in range(1, SIDE):
+            pl.semaphore_signal(semaphore, inc=1, device_id=along_first(place), device_id_type=MESH)
+            pl.semaphore_signal(semaphore, inc=1, device_id=along_second(place), device_id_type=MESH)
+        pl.semaphore_signal(semaphore, inc=1, device_id=partner, device_id_type=MESH)
+
     barrier = pltpu.get_barrier_semaphore()
-    for place in range(1, SIDE):
-        pl.semaphore_signal(barrier, inc=1, device_id=along_first(place), device_id_type=MESH)
-        pl.semaphore_signal(barrier, inc=1, device_id=along_second(place), device_id_type=MESH)
-    pl.semaphore_signal(barrier, inc=1, device_id=partner, device_id_type=MESH)
+
+    @pl.when(jnp.logical_not(is_lead))
+    def _():
+        signal_peers(barrier)
+
+    def await_lead(who):
+        @pl.when(who & jnp.logical_not(is_lead))
+        def _():
+            pl.semaphore_wait(lead_sem, 1)
 
     def send(src, dst, send_sem, recv_sem, to):
         copy = pltpu.make_async_remote_copy(
@@ -117,6 +128,33 @@
     ]
     for load in loads:
         load.start()
+
+    tok_load.wait()
+    values = tok_in[...].astype(F32)
+    scale = lax.rsqrt(jnp.mean(values * values, axis=-1, keepdims=True) + EPSILON)
+    toks[0] = (tok_in[:, own].astype(F32) * scale * gain_ref[:, own]).astype(BF)
+
+    pl.semaphore_wait(barrier, peer_count - knows_lead.astype(jnp.int32))
+
+    @pl.when(is_lead)
+    def _():
+        signal_peers(lead_sem)
+
+    await_lead(in_lead_row)
+
+    def piece(p):
+        return pl.ds(p * (rows // RING_CUT), rows // RING_CUT)
+
+    def pass_on(place, to_place, p):
+        backward = place % 2 == 1 if place else to_place % 2 == 1
+        send(
+            toks.at[place, piece(p)], toks.at[to_place, piece(p)],
+            ag_send.at[to_place, p], ag_recv.at[to_place, p], along_first(2 if backward else 1),
+        )
+
+    for p in range(RING_CUT):
+        pass_on(0, 1, p)
+        pass_on(0, 2, p)
 
     lanes = 2 * rows
     experts = SIDE * SIDE
@@ -155,31 +193,10 @@
     meta_out[:, 1] = gates.reshape(SIDE, SIDE, lanes)
     meta[0] = meta_out[0]
 
-    tok_load.wait()
-    values = tok_in[...].astype(F32)
-    scale = lax.rsqrt(jnp.mean(values * values, axis=-1, keepdims=True) + EPSILON)
-    toks[0] = (tok_in[:, own].astype(F32) * scale * gain_ref[:, own]).astype(BF)
-
+    for place in range(1, SIDE):
+        send(meta_out.at[place], meta.at[BACK[place]], meta_send.at[place], meta_recv.at[BACK[place]], along_first(place))
     accg[...] = jnp.zeros_like(accg)
     accu[...] = jnp.zeros_like(accu)
-
-    pl.semaphore_wait(barrier, 2 * (SIDE - 1) + 1)
-
-    def piece(p):
-        return pl.ds(p * (rows // RING_CUT), rows // RING_CUT)
-
-    def pass_on(place, to_place, p):
-        backward = place % 2 == 1 if place else to_place % 2 == 1
-        send(
-            toks.at[place, piece(p)], toks.at[to_place, piece(p)],
-            ag_send.at[to_place, p], ag_recv.at[to_place, p], along_first(2 if backward else 1),
-        )
-
-    for place in range(1, SIDE):
-        send(meta_out.at[place], meta.at[BACK[place]], meta_send.at[place], meta_recv.at[BACK[place]], along_first(place))
-    for p in range(RING_CUT):
-        pass_on(0, 1, p)
-        pass_on(0, 2, p)
 
     slot_iota = (lax.broadcasted_iota(jnp.int32, (SIDE * cap, lanes), 0) % cap).astype(F32)
 
@@ -196,6 +213,13 @@
                     onward = next_outward(s, p)
                     if onward:
                         pass_on(s, onward, p)
+
+    up = (SIDE - second) % SIDE
+    beyond = up // (SIDE // 2 + 1)
+    lead_place = (1 - beyond) * (2 * up - 1) + beyond * 2 * (SIDE - up)
+    my_place = lead_place + 2 * (lead_place % 2) - 1 - lead_place // FAR
+    follows = (in_lead_column & jnp.logical_not(is_lead)).astype(jnp.int32)
+    lead_place = lead_place * follows - (1 - follows)
 
     def pick_and_send(s):
         if s > 0:
@@ -206,7 +230,10 @@
         sel[s] = picked
         xin[s, 0] = picked[0]
         for place in range(SIDE - 1, 0, -1):
-            send(sel.at[s, place], xin.at[s, BACK[place]], sel_send.at[s], xin_recv.at[s], along_second(place))
+
+            @pl.when(place != lead_place)
+            def _():
+                send(sel.at[s, place], xin.at[s, BACK[place]], sel_send.at[s], xin_recv.at[s], along_second(place))
 
     def take_own(s):
         wait_bytes(xin.at[s, pl.ds(1, SIDE - 1)], xin_recv.at[s])
@@ -221,21 +248,38 @@
         accg[:, s] += jnp.dot(block, wg[1], preferred_element_type=F32).reshape(SIDE, cap, hidden)
         accu[:, s] += jnp.dot(block, wu[1], preferred_element_type=F32).reshape(SIDE, cap, hidden)
 
-    for places, owns, others in OUTWARD:
+    def activate(*at):
+        gate_acts = accg[at]
+        hid[at] = (gate_acts / (1.0 + jnp.exp(-gate_acts)) * accu[at]).astype(BF)
+
+    receive((1, 2))
+    for s in (0, 1, 2):
+        pick_and_send(s)
+    for places in ((3, 4), (5, 6), (FAR,)):
         receive(places)
         for s in places:
             pick_and_send(s)
-        if places == (3, 4):
-            for load in loads:
-                load.wait()
-        for s in owns:
-            take_own(s)
-        for s in others:
-            take_other(s)
-
-    for s in range(SIDE):
-        gate_acts = accg[s]
-        hid[s] = (gate_acts / (1.0 + jnp.exp(-gate_acts)) * accu[s]).astype(BF)
+    await_lead(in_lead_column)
+
+    @pl.when(lead_place > 0)
+    def _():
+        for s in range(SIDE):
+            send(sel.at[s, lead_place], xin.at[s, my_place], sel_send.at[s], xin_recv.at[s], (grp, 0, core))
+
+    for load in loads:
+        load.wait()
+    await_lead(beside_lead)
+    take_own(0)
+    for s in range(1, FAR):
+        take_own(s)
+        take_other(s - 1)
+    take_other(FAR - 1)
+    for s in range(FAR):
+        activate(s, pl.ds(0, FAR))
+    take_own(FAR)
+    take_other(FAR)
+    activate(FAR)
+    activate(pl.ds(0, FAR), FAR)
 
     def multiply_down(s):
         theirs = hid[:, s].reshape(SIDE * cap, hidden)
@@ -353,7 +397,8 @@
             dma((SIDE, SUM_CUT)),
             dma((SIDE, SUM_CUT)),
         ]
-        + [dma((SIDE,)) for _ in range(10)],
+        + [dma((SIDE,)) for _ in range(10)]
+        + [pltpu.SemaphoreType.REGULAR],
         compiler_params=pltpu.CompilerParams(
             collective_id=0, has_side_effects=True, vmem_limit_bytes=60 * 1024 * 1024
         ),

time: 96.2 us -> 92.5 us (0.962)
  Pallas kernels: 94.4 us -> 90.7 us
    pallas_call x1, Pallas kernels: 94.4 us -> 90.7 us  [on_device(): pl.pallas_call(moe_kernel, out_shape=jax.ShapeDtypeStruct((rows, part), F...]
where the time goes in v3:
time: 92.5 us; the launch traced here: 92.3 us
  Pallas kernels  90.7 us (98%)
  other arithmetic  1.62 us (2%)
    pallas_call x1, Pallas kernels, on_device(): pl.pallas_call(moe_kernel, out_shape=jax.ShapeDtypeStruct((rows, part), F...  90.7 us

profile of v3, /device:TPU:513, one launch (start us, length us, event | category | flops | bytes accessed | tf_op | source)
XLA Modules:
  0.0 92.3 jit_solution(8101352611002001206)
XLA Ops:
  0.0 90.7 %moe.1 = f32[64,1024]{1,0:T(8,128)} custom-call(s32[8,64]{1,0:T(8,128)} %bitcast.5, f32[8,64]{1,0:T(8,128)} %bitcast.6, f32[8,64]{1,0:T(8,128)} %bitcast.7, bf16[64,2048]{1,0:T(8,128)(2,1)} %tokens_hbm.1, f32[1,2048]{1,0:T(1,128)} %bitcast.4, bf16[1,2048,512]{2,1,0:T(8,128)(2,1)} %gate_hbm.1, bf16[1,2048,512]{2,1,0:T(8,128)(2,1)} %up_hbm.1, ...), custom_call_target="tpu_custom_call" | custom-call | tf_op jit(solution)/shard_map/moe/pallas_call | solution.py:358
  90.7 1.6 %convert_element_type.3 = bf16[64,1024]{1,0:T(8,128)(2,1)} convert(f32[64,1024]{1,0:T(8,128)} %moe.1) | non-fusion elementwise | flops 65536 | bytes 393216 | tf_op jit(solution)/shard_map/convert_element_type | solution.py:410

commit v4 on v3

--- a/solution.py
+++ b/solution.py
@@ -23,6 +23,7 @@
 INWARD = [s for places in INWARD_GROUPS for s in places]
 RING_CUT = 4
 SUM_CUT = 2
+HELD_BACK = 5
 
 
 def next_outward(place, p):
@@ -220,6 +221,7 @@
     my_place = lead_place + 2 * (lead_place % 2) - 1 - lead_place // FAR
     follows = (in_lead_column & jnp.logical_not(is_lead)).astype(jnp.int32)
     lead_place = lead_place * follows - (1 - follows)
+    lead = (grp, 0, core)
 
     def pick_and_send(s):
         if s > 0:
@@ -231,52 +233,76 @@
         xin[s, 0] = picked[0]
         for place in range(SIDE - 1, 0, -1):
 
-            @pl.when(place != lead_place)
-            def _():
+            def send_rows():
                 send(sel.at[s, place], xin.at[s, BACK[place]], sel_send.at[s], xin_recv.at[s], along_second(place))
 
-    def take_own(s):
-        wait_bytes(xin.at[s, pl.ds(1, SIDE - 1)], xin_recv.at[s])
-        send(xin.at[s], xoth.at[:, s], xo_send.at[s], xo_recv.at[s], partner)
-        block = xin[s].reshape(SIDE * cap, part)
-        accg[s] += jnp.dot(block, wg[0], preferred_element_type=F32).reshape(SIDE, cap, hidden)
-        accu[s] += jnp.dot(block, wu[0], preferred_element_type=F32).reshape(SIDE, cap, hidden)
-
-    def take_other(s):
-        wait_bytes(xoth.at[:, s], xo_recv.at[s])
-        block = xoth[:, s].reshape(SIDE * cap, part)
-        accg[:, s] += jnp.dot(block, wg[1], preferred_element_type=F32).reshape(SIDE, cap, hidden)
-        accu[:, s] += jnp.dot(block, wu[1], preferred_element_type=F32).reshape(SIDE, cap, hidden)
+            if s < HELD_BACK:
+                pl.when(place != lead_place)(send_rows)
+            else:
+                send_rows()
+
+    def multiply_in(block, at, half):
+        for acc, weights in ((accg, wg), (accu, wu)):
+            acts = jnp.dot(block.reshape(-1, part), weights[half], preferred_element_type=F32)
+            acc[at] += acts.reshape(block.shape[:-1] + (hidden,))
+
+    def take_own(s, count=1):
+        for one in range(s, s + count):
+            wait_bytes(xin.at[one, pl.ds(1, SIDE - 1)], xin_recv.at[one])
+            send(xin.at[one], xoth.at[:, one], xo_send.at[one], xo_recv.at[one], partner)
+        multiply_in(xin[s : s + count], (pl.ds(s, count),), 0)
+
+    def take_other(s, count=1):
+        for one in range(s, s + count):
+            wait_bytes(xoth.at[:, one], xo_recv.at[one])
+        multiply_in(xoth[:, s : s + count], (slice(None), pl.ds(s, count)), 1)
 
     def activate(*at):
         gate_acts = accg[at]
         hid[at] = (gate_acts / (1.0 + jnp.exp(-gate_acts)) * accu[at]).astype(BF)
 
+    early = in_lead_row & jnp.logical_not(is_lead)
+
+    def when(condition, *work):
+        @pl.when(condition)
+        def _():
+            for take, s in work:
+                take(s, 2)
+
     receive((1, 2))
     for s in (0, 1, 2):
         pick_and_send(s)
-    for places in ((3, 4), (5, 6), (FAR,)):
-        receive(places)
-        for s in places:
-            pick_and_send(s)
+    receive((3, 4))
+    for s in (3, 4):
+        pick_and_send(s)
     await_lead(in_lead_column)
 
     @pl.when(lead_place > 0)
     def _():
-        for s in range(SIDE):
-            send(sel.at[s, lead_place], xin.at[s, my_place], sel_send.at[s], xin_recv.at[s], (grp, 0, core))
+        for s in range(HELD_BACK):
+            send(sel.at[s, lead_place], xin.at[s, my_place], sel_send.at[s], xin_recv.at[s], lead)
 
     for load in loads:
         load.wait()
+    when(early, (take_own, 0))
+    receive((5, 6))
+    for s in (5, 6):
+        pick_and_send(s)
+    when(early, (take_own, 2), (take_other, 0))
+    when(is_lead, (take_own, 0))
+    receive((FAR,))
+    pick_and_send(FAR)
     await_lead(beside_lead)
-    take_own(0)
-    for s in range(1, FAR):
-        take_own(s)
-        take_other(s - 1)
+    when(jnp.logical_not(in_lead_row), (take_own, 0))
+    when(jnp.logical_not(early), (take_own, 2), (take_other, 0))
+    take_own(4, 2)
+    take_other(2, 2)
+    take_own(FAR - 1)
+    take_other(4, 2)
     take_other(FAR - 1)
+    take_own(FAR)
     for s in range(FAR):
         activate(s, pl.ds(0, FAR))
-    take_own(FAR)
     take_other(FAR)
     activate(FAR)
     activate(pl.ds(0, FAR), FAR)
@@ -357,7 +383,7 @@
     blocks = (SIDE, SIDE, cap, part)
     result = pl.pallas_call(
         moe_kernel,
-        out_shape=jax.ShapeDtypeStruct((rows, part), F32),
+        out_shape=pltpu.VMEM((rows, part), F32),
         in_specs=[
             pl.BlockSpec(memory_space=pltpu.VMEM),
             pl.BlockSpec(memory_space=pltpu.VMEM),

time: 92.5 us -> 89.2 us (0.964)
  Pallas kernels: 90.7 us -> 88.4 us
  other arithmetic: 1.62 us -> 0.67 us
    pallas_call x1, Pallas kernels: 90.7 us -> 88.4 us  [on_device(): pl.pallas_call(moe_kernel, out_shape=pltpu.VMEM((rows, part), F32), in_sp...]
    convert_element_type x1, other arithmetic: 1.62 us -> 0.67 us  [on_device(): return result.astype(BF)]
where the time goes in v4:
time: 89.2 us; the launch traced here: 89 us
  Pallas kernels  88.4 us (99%)
    pallas_call x1, Pallas kernels, on_device(): pl.pallas_call(moe_kernel, out_shape=pltpu.VMEM((rows, part), F32), in_sp...  88.4 us

profile of v4, /device:TPU:513, one launch (start us, length us, event | category | flops | bytes accessed | tf_op | source)
XLA Modules:
  0.0 89.0 jit_solution(17690273079431954664)
XLA Ops:
  0.0 88.4 %moe.1 = f32[64,1024]{1,0:T(8,128)S(1)} custom-call(s32[8,64]{1,0:T(8,128)} %bitcast.5, f32[8,64]{1,0:T(8,128)} %bitcast.6, f32[8,64]{1,0:T(8,128)} %bitcast.7, bf16[64,2048]{1,0:T(8,128)(2,1)} %tokens_hbm.1, f32[1,2048]{1,0:T(1,128)} %bitcast.4, bf16[1,2048,512]{2,1,0:T(8,128)(2,1)} %gate_hbm.1, bf16[1,2048,512]{2,1,0:T(8,128)(2,1)} %up_hbm.1, ...), custom_call_target="tpu_custom_call" | custom-call | tf_op jit(solution)/shard_map/moe/pallas_call | solution.py:384
  88.4 0.7 convert_element_type.3

commit v5 on v4

--- a/solution.py
+++ b/solution.py
@@ -100,6 +100,11 @@
     def _():
         signal_peers(barrier)
 
+    @pl.when(is_lead)
+    def _():
+        pl.semaphore_wait(barrier, peer_count)
+        signal_peers(lead_sem)
+
     def await_lead(who):
         @pl.when(who & jnp.logical_not(is_lead))
         def _():
@@ -135,13 +140,20 @@
     scale = lax.rsqrt(jnp.mean(values * values, axis=-1, keepdims=True) + EPSILON)
     toks[0] = (tok_in[:, own].astype(F32) * scale * gain_ref[:, own]).astype(BF)
 
-    pl.semaphore_wait(barrier, peer_count - knows_lead.astype(jnp.int32))
-
-    @pl.when(is_lead)
+    @pl.when(jnp.logical_not(is_lead))
     def _():
-        signal_peers(lead_sem)
-
-    await_lead(in_lead_row)
+        pl.semaphore_wait(barrier, peer_count - knows_lead.astype(jnp.int32))
+
+    def lead_at(up, follows):
+        beyond = up // (SIDE // 2 + 1)
+        place = (1 - beyond) * (2 * up - 1) + beyond * 2 * (SIDE - up)
+        back = place + 2 * (place % 2) - 1 - place // FAR
+        follows = (follows & jnp.logical_not(is_lead)).astype(jnp.int32)
+        return place * follows - (1 - follows), back
+
+    lead_slot, my_slot = lead_at((SIDE - first) % SIDE, in_lead_row)
+    lead_place, my_place = lead_at((SIDE - second) % SIDE, in_lead_column)
+    lead = (grp, 0, core)
 
     def piece(p):
         return pl.ds(p * (rows // RING_CUT), rows // RING_CUT)
@@ -154,8 +166,8 @@
         )
 
     for p in range(RING_CUT):
-        pass_on(0, 1, p)
-        pass_on(0, 2, p)
+        for place in (1, 2):
+            pl.when(lead_slot != BACK[place])(functools.partial(pass_on, 0, place, p))
 
     lanes = 2 * rows
     experts = SIDE * SIDE
@@ -194,8 +206,11 @@
     meta_out[:, 1] = gates.reshape(SIDE, SIDE, lanes)
     meta[0] = meta_out[0]
 
+    def send_meta(place, slot, to):
+        send(meta_out.at[place], meta.at[slot], meta_send.at[place], meta_recv.at[slot], to)
+
     for place in range(1, SIDE):
-        send(meta_out.at[place], meta.at[BACK[place]], meta_send.at[place], meta_recv.at[BACK[place]], along_first(place))
+        pl.when(lead_slot != place)(functools.partial(send_meta, place, BACK[place], along_first(place)))
     accg[...] = jnp.zeros_like(accg)
     accu[...] = jnp.zeros_like(accu)
 
@@ -214,14 +229,6 @@
                     onward = next_outward(s, p)
                     if onward:
                         pass_on(s, onward, p)
-
-    up = (SIDE - second) % SIDE
-    beyond = up // (SIDE // 2 + 1)
-    lead_place = (1 - beyond) * (2 * up - 1) + beyond * 2 * (SIDE - up)
-    my_place = lead_place + 2 * (lead_place % 2) - 1 - lead_place // FAR
-    follows = (in_lead_column & jnp.logical_not(is_lead)).astype(jnp.int32)
-    lead_place = lead_place * follows - (1 - follows)
-    lead = (grp, 0, core)
 
     def pick_and_send(s):
         if s > 0:
@@ -269,7 +276,26 @@
             for take, s in work:
                 take(s, 2)
 
+    def greet_lead(near):
+        known = in_lead_row & jnp.logical_not(is_lead)
+        mine = known & ((lead_slot < 3) if near else (lead_slot > 2))
+        await_lead(mine)
+
+        @pl.when(mine)
+        def _():
+            send_meta(lead_slot, my_slot, lead)
+
+        if near:
+            for place in (1, 2):
+
+                @pl.when(lead_slot == BACK[place])
+                def _():
+                    for p in range(RING_CUT):
+                        pass_on(0, place, p)
+
+    greet_lead(True)
     receive((1, 2))
+    greet_lead(False)
     for s in (0, 1, 2):
         pick_and_send(s)
     receive((3, 4))

time: 89.2 us -> 89.9 us (level)
  no operation moved by 1% of the time
where the time goes in v5:
time: 89.9 us; the launch traced here: 89.8 us
  Pallas kernels  89.1 us (99%)
    pallas_call x1, Pallas kernels, on_device(): pl.pallas_call(moe_kernel, out_shape=pltpu.VMEM((rows, part), F32), in_sp...  89.1 us

profile of v5, /device:TPU:513, one launch (start us, length us, event | category | flops | bytes accessed | tf_op | source)
XLA Modules:
  0.0 89.8 jit_solution(3844594239075499482)
XLA Ops:
  0.0 89.1 %moe.1 = f32[64,1024]{1,0:T(8,128)S(1)} custom-call(s32[8,64]{1,0:T(8,128)} %bitcast.5, f32[8,64]{1,0:T(8,128)} %bitcast.6, f32[8,64]{1,0:T(8,128)} %bitcast.7, bf16[64,2048]{1,0:T(8,128)(2,1)} %tokens_hbm.1, f32[1,2048]{1,0:T(1,128)} %bitcast.4, bf16[1,2048,512]{2,1,0:T(8,128)(2,1)} %gate_hbm.1, bf16[1,2048,512]{2,1,0:T(8,128)(2,1)} %up_hbm.1, ...), custom_call_target="tpu_custom_call" | custom-call | tf_op jit(solution)/shard_map/moe/pallas_call | solution.py:410
  89.1 0.7 convert_element_type.3

commit v6 on v4

--- a/solution.py
+++ b/solution.py
@@ -21,7 +21,7 @@
 FAR = SIDE - 1
 INWARD_GROUPS = [(FAR,), (5, 6), (3, 4), (1, 2), (0,)]
 INWARD = [s for places in INWARD_GROUPS for s in places]
-RING_CUT = 4
+RING_CUT = 8
 SUM_CUT = 2
 HELD_BACK = 5
 

time: 89.2 us -> 89.9 us (level)
  no operation moved by 1% of the time
where the time goes in v6:
time: 89.9 us; the launch traced here: 89.7 us
  Pallas kernels  89 us (99%)
    pallas_call x1, Pallas kernels, on_device(): pl.pallas_call(moe_kernel, out_shape=pltpu.VMEM((rows, part), F32), in_sp...  89 us

profile of v6, /device:TPU:513, one launch (start us, length us, event | category | flops | bytes accessed | tf_op | source)
XLA Modules:
  0.0 89.7 jit_solution(3789087219342247760)
XLA Ops:
  0.0 89.0 %moe.1 = f32[64,1024]{1,0:T(8,128)S(1)} custom-call(s32[8,64]{1,0:T(8,128)} %bitcast.5, f32[8,64]{1,0:T(8,128)} %bitcast.6, f32[8,64]{1,0:T(8,128)} %bitcast.7, bf16[64,2048]{1,0:T(8,128)(2,1)} %tokens_hbm.1, f32[1,2048]{1,0:T(1,128)} %bitcast.4, bf16[1,2048,512]{2,1,0:T(8,128)(2,1)} %gate_hbm.1, bf16[1,2048,512]{2,1,0:T(8,128)(2,1)} %up_hbm.1, ...), custom_call_target="tpu_custom_call" | custom-call | tf_op jit(solution)/shard_map/moe/pallas_call | solution.py:384
  89.1 0.7 convert_element_type.3
